TPU v7x, 512 devices: a whole 4x8x8 slice. The times are simulated.
512 devices in a mesh: ep: 32 (over z, x), tp: 16 (over y, core).
Axes of the slice: x: 4, y: 8, z: 8, core: 2. Of those that a mesh axis runs over, the one named last changes fastest.
Arguments:
- pool_input: bfloat16 [8192, 2048], P('ep', 'tp'), may hold values from -6 to 6
- pool_map: bfloat16 [16, 128, 128], replicated, may hold values from -0.5 to 0.5
- pool_scale: float32 [2048], replicated, may hold values from 0.1 to 1.9
- out_proj: bfloat16 [2048, 4096], P('tp'), may hold values from -0.125 to 0.125
- moe_input: bfloat16 [4096, 4096], P('ep'), may hold values from -6 to 6
- norm_gain: float32 [4096], replicated, may hold values from 0.1 to 1.9
- routes: int32 [4096, 4], P('ep'), may hold values from 0 to 31, all different within a row; in each aligned block of 128 rows (0 to 127, 128 to 255, ...) at most 24 rows name the same one
- route_weights: float32 [4096, 4], P('ep'), may hold values from 0.1 to 1
- expert_gate: bfloat16 [32, 4096, 1024], P('ep', None, 'tp'), may hold values from -0.09375 to 0.09375
- expert_up: bfloat16 [32, 4096, 1024], P('ep', None, 'tp'), may hold values from -0.09375 to 0.09375
- expert_down: bfloat16 [32, 1024, 4096], P('ep', None, 'tp'), may hold values from -0.1875 to 0.1875
- shared_gate: bfloat16 [4096, 512], P(None, 'tp'), may hold values from -0.09375 to 0.09375
- shared_up: bfloat16 [4096, 512], P(None, 'tp'), may hold values from -0.09375 to 0.09375
- shared_down: bfloat16 [512, 4096], P('tp'), may hold values from -0.25 to 0.25
Outputs:
- mixer_output: bfloat16 [8192, 4096], P('ep', 'tp')
- moe_output: bfloat16 [4096, 4096], P('ep', 'tp')
Inputs may be any that keep to these rules, and one draw needn't show every extreme that they name: `routes`: each row names 4 different experts. In each aligned block of 128 rows no expert is named by more than 24 rows, a bound that some block reaches.
All inputs are finite; a program needn't handle non-finite values.
Results may differ from a plain program's by a relative error of at most 0.017.
Values may be sent and summed in bfloat16 or wider, within the bound.
No kernel may reach another device: no remote copies, remote signals or barrier semaphores. Data moves between devices by JAX's collectives and lax.ppermute only.
A program may use at most 64 MiB of HBM per device.

v0:
```python
import jax
import jax.numpy as jnp
from jax import lax
from jax.sharding import PartitionSpec as P

windows = (2, 4, 8, 16)
reach_back = 15
eps = 1e-05


def passed_along(block, axis, distance):
    devices = range(lax.axis_size(axis))
    route = [(i - distance, i) for i in devices if i - distance in devices]
    return lax.ppermute(block, axis, route)


def sent_to_all(x, axis):
    devices = lax.axis_size(axis)
    return lax.all_to_all(jnp.broadcast_to(x[None], (devices, *x.shape)), axis, 0, 0, tiled=True)


def joined_along(pieces, dim):
    shape = list(pieces.shape[1:])
    shape[dim] *= pieces.shape[0]
    return jnp.moveaxis(pieces, 0, dim).reshape(shape)


def gathered_copies(x, axis, dim):
    pieces = sent_to_all(x, axis)
    return joined_along(pieces, dim)


def in_one_piece(arrays, axis, dim, along):
    both = jnp.concatenate(arrays, axis=along)
    out, at, done = (lax.psum_scatter(both, axis, scatter_dimension=dim, tiled=True), 0, [])
    for a in arrays:
        done.append(lax.slice_in_dim(out, at, at + a.shape[along], axis=along))
        at += a.shape[along]
    return tuple(done)


def pool_branch(pool_input, pool_map, pool_scale, out_proj):
    row_count = pool_input.shape[0]
    channels = pool_input.shape[1]
    group_dim = pool_map.shape[1]
    local_groups = channels // group_dim
    tp_rank = lax.axis_index("tp")
    ep_rank = lax.axis_index("ep")
    earlier_rows = passed_along(pool_input[row_count - reach_back :], "ep", 1)
    values = pool_input.astype(jnp.float32)
    extended = jnp.concatenate([earlier_rows.astype(jnp.float32), values], axis=0)
    position = (ep_rank * row_count + jnp.arange(row_count, dtype=jnp.int32)).astype(jnp.float32)
    group_ids = tp_rank * local_groups + jnp.arange(channels, dtype=jnp.int32) // group_dim
    group_kind = group_ids % 4
    running = jnp.zeros((row_count, channels), jnp.float32)
    pooled = -values
    for lag_step in range(reach_back + 1):
        running = running + extended[reach_back - lag_step : reach_back - lag_step + row_count]
        if lag_step + 1 in windows:
            kind_id = windows.index(lag_step + 1)
            counts = jnp.minimum(position + 1.0, float(lag_step + 1))
            select = (group_kind == kind_id).astype(jnp.float32)
            pooled = pooled + select[None, :] * running / counts[:, None]
    pooled = pooled.astype(jnp.bfloat16)
    my_maps = lax.dynamic_slice_in_dim(pool_map, tp_rank * local_groups, local_groups, 0)
    my_scale = lax.dynamic_slice_in_dim(pool_scale, tp_rank * channels, channels, 0)
    mapped = jnp.einsum(
        "rgc,gcd->rgd",
        pooled.reshape(row_count, local_groups, group_dim),
        my_maps,
        preferred_element_type=jnp.float32,
    )
    group_out = (mapped.reshape(row_count, channels) * my_scale[None, :]).astype(jnp.bfloat16)
    return jnp.dot(group_out, out_proj, preferred_element_type=jnp.float32)


def dispatch_rows(routes, expert_count, capacity):
    tok_count, top_count = routes.shape
    flat_ids = routes.reshape(tok_count * top_count)
    one_hot = (flat_ids[:, None] == jnp.arange(expert_count, dtype=jnp.int32)[None, :]).astype(
        jnp.int32
    )
    earlier = jnp.cumsum(one_hot, axis=0) - one_hot
    slot_ids = jnp.sum(earlier * one_hot, axis=1)
    return (flat_ids * capacity + slot_ids).reshape(tok_count, top_count)


def per_device(
    pool_input,
    pool_map,
    pool_scale,
    out_proj,
    moe_input,
    norm_gain,
    routes,
    route_weights,
    expert_gate,
    expert_up,
    expert_down,
    shared_gate,
    shared_up,
    shared_down,
):
    mixer_part = pool_branch(pool_input, pool_map, pool_scale, out_proj)
    values = moe_input.astype(jnp.float32)
    centre = values - jnp.mean(values, axis=1, keepdims=True)
    variance = jnp.mean(centre * centre, axis=1, keepdims=True)
    normed = (centre * lax.rsqrt(variance + eps) * norm_gain[None, :]).astype(jnp.bfloat16)
    expert_count = lax.axis_size("ep")
    tok_count = moe_input.shape[0]
    top_count = routes.shape[1]
    capacity = (3 * tok_count * top_count + 2 * expert_count - 1) // (2 * expert_count)
    slot_index = dispatch_rows(routes, expert_count, capacity)
    buffer_len = expert_count * capacity
    targets = jnp.arange(buffer_len, dtype=jnp.int32)[:, None]
    placing = jnp.zeros((buffer_len, tok_count), jnp.float32)
    for top_step in range(top_count):
        placing = placing + (targets == slot_index[None, :, top_step]).astype(jnp.float32)
    outgoing = jnp.dot(
        placing.astype(jnp.bfloat16), normed, preferred_element_type=jnp.float32
    ).astype(jnp.bfloat16)
    gate_weight = expert_gate[0]
    up_weight = expert_up[0]
    down_weight = expert_down[0]
    tp_rank = lax.axis_index("tp")
    slice_width = outgoing.shape[1] // lax.axis_size("tp")
    my_slice = lax.dynamic_slice_in_dim(outgoing, tp_rank * slice_width, slice_width, 1)
    arrived = lax.all_to_all(my_slice, "ep", split_axis=0, concat_axis=0, tiled=True)
    shard_cols = lax.all_gather(arrived, "tp", axis=1, tiled=True)
    gate_val = jnp.dot(shard_cols, gate_weight, preferred_element_type=jnp.float32)
    up_val = jnp.dot(shard_cols, up_weight, preferred_element_type=jnp.float32)
    hidden = (jax.nn.silu(gate_val) * up_val).astype(jnp.bfloat16)
    expert_result = jnp.dot(
        gathered_copies(hidden, "tp", 1), down_weight, preferred_element_type=jnp.float32
    ).astype(jnp.bfloat16)
    returned = lax.all_to_all(expert_result, "ep", split_axis=0, concat_axis=0, tiled=True)
    routed = jnp.zeros((tok_count, returned.shape[1]), jnp.float32)
    for top_step in range(top_count):
        picked = returned[slot_index[:, top_step]].astype(jnp.float32)
        routed = routed + route_weights[:, top_step, None] * picked
    shared_gate_val = jnp.dot(normed, shared_gate, preferred_element_type=jnp.float32)
    shared_up_val = jnp.dot(normed, shared_up, preferred_element_type=jnp.float32)
    shared_hidden = (jax.nn.silu(shared_gate_val) * shared_up_val).astype(jnp.bfloat16)
    shared_part = jnp.dot(shared_hidden, shared_down, preferred_element_type=jnp.float32)
    mixer_sum, shared_sum = tuple(
        (
            part.astype(jnp.float32)
            for part in in_one_piece(
                (mixer_part.astype(jnp.bfloat16), shared_part.astype(jnp.bfloat16)), "tp", 1, 0
            )
        )
    )
    return (mixer_sum.astype(jnp.bfloat16), (routed + shared_sum).astype(jnp.bfloat16))


def solution(mesh):
    return jax.shard_map(
        per_device,
        mesh=mesh,
        in_specs=(
            P("ep", "tp"),
            P(),
            P(),
            P("tp", None),
            P("ep", None),
            P(),
            P("ep", None),
            P("ep", None),
            P("ep", None, "tp"),
            P("ep", None, "tp"),
            P("ep", None, "tp"),
            P(None, "tp"),
            P(None, "tp"),
            P("tp", None),
        ),
        out_specs=(P("ep", "tp"), P("ep", "tp")),
        check_vma=False,
    )
```

profile of v0, /device:TPU:1, one launch (start us, length us, event | category | flops | bytes accessed | tf_op | source)
XLA Modules:
  0.0 197.1 jit_solution(10955667984421792337)
XLA Ops:
  7.2 0.9 copy.27
  8.4 1.2 reduce-window.6
  9.6 0.2 slice_reduce_fusion
  9.8 0.1 fusion.55
  10.0 0.1 reduce_sum.32
  10.1 0.7 multiply_add_fusion
  10.8 1.5 convert_reduce_fusion
  12.3 0.4 fusion.2
  12.8 1.9 fusion.13
  14.8 27.4 %all_to_all.29 = bf16[32,24,256]{2,1,0:T(8,128)(2,1)} all-to-all(bf16[32,24,256]{2,1,0:T(8,128)(2,1)S(1)} %bitcast.88), channel_id=1, replica_groups=mesh['ep'=32,'tp'=16] {'ep'}, dimensions={0} | all-to-all | bytes 786432 | tf_op jit(solution)/shard_map/all_to_all | solution.py:128
  42.3 2.3 %collective-permute-start = (bf16[15,128]{1,0:T(8,128)(2,1)S(1)}, bf16[15,128]{1,0:T(8,128)(2,1)S(1)}, u32[]{:S(2)}, u32[]{:S(2)}) collective-permute-start(bf16[15,128]{1,0:T(8,128)(2,1)S(1)} %slice.88), channel_id=1, source_target_pairs={{0,16},{16,32},{32,48},{48,64},{64,80},{80,96},{96,112},{112,128},... | collective-permute-start | bytes 11528 | tf_op jit(solution)/shard_map/ppermute | solution.py:14
  44.7 0.5 compare_convert_fusion
  45.2 0.5 fusion.102
  45.7 2.4 %convolution_convert_fusion.1 = bf16[128,4096]{1,0:T(8,128)(2,1)S(1)} fusion(bf16[32,4096]{1,0:T(8,128)(2,1)S(1)} %copy-done.5, bf16[4096,32]{0,1:T(8,128)(2,1)} %param.26, f32[128,32]{0,1:T(8,128)S(1)} %fusion.102, bf16[128,4096]{1,0:T(8,128)(2,1)S(1)} %copy-done.2, f32[4096]{0:T(1024)S(1)} %copy-done.7, f32[128]{0:T(128)S(1)} %add_rsqrt_fusion, ...), kind=kOutput, calls=%fused_computation.5 | convolution fusion | flops 70279168 | bytes 2655232 | tf_op jit(solution)/shard_map/dot_general | solution.py:144
  48.2 0.8 dynamic_slice.10
  49.0 3.3 %convolution_convert_fusion = bf16[256,4096]{1,0:T(8,128)(2,1)} fusion(bf16[128,4096]{1,0:T(8,128)(2,1)S(1)} %copy-done, f32[256,128]{1,0:T(8,128)S(1)} %convert_element_type.122, f32[15,128]{1,0:T(8,128)S(1)} %convert_element_type.124, f32[128]{0:T(128)S(1)} %dynamic_slice.10, f32[256]{0:T(256)S(1)} %get-tuple-element.18, f32[128]{0:T(128)} %get-tuple-element.14, ...), kind=kOutput, calls=%fused_computation.4 | convolution fusion | flops 279379968 | bytes 3323908 | tf_op jit(solution)/shard_map/dot_general | solution.py:74
  52.2 3.6 %pad_maximum_fusion = bf16[384,4096]{1,0:T(8,128)(2,1)} fusion(bf16[128,4096]{1,0:T(8,128)(2,1)S(1)} %convolution_convert_fusion.1, bf16[256,4096]{1,0:T(8,128)(2,1)} %convolution_convert_fusion), kind=kLoop, calls=%fused_computation.6 | loop fusion | flops 6291456 | bytes 6291456 | tf_op jit(solution)/shard_map/concatenate | solution.py:34
  55.8 44.0 %all-gather.2.cloned.1.call-done = bf16[768,4096]{1,0:T(8,128)(2,1)} async-done(((bf16[768,256]{1,0:T(8,128)(2,1)}), bf16[768,4096]{1,0:T(8,128)(2,1)}) %all-gather.2.cloned.1.call-update) | async-done | bytes 6291472 | tf_op jit(solution)/shard_map/all_gather | solution.py:129
  99.8 5.0 %fusion.11 = f32[768,64]{0,1:T(8,128)S(1)} fusion(bf16[768,4096]{1,0:T(8,128)(2,1)} %all-gather.2.cloned.1.call-done, bf16[1,4096,64]{1,2,0:T(8,128)(2,1)S(1)} %copy-done.4), kind=kOutput, calls=%fused_computation.39 | convolution fusion | flops 402653184 | bytes 7012352 | tf_op jit(solution)/shard_map/dot_general | solution.py:130
  104.8 2.1 %fusion.5 = bf16[768,64]{0,1:T(8,128)(2,1)S(1)} fusion(bf16[768,4096]{1,0:T(8,128)(2,1)S(1)} %copy-done.1, bf16[1,4096,64]{1,2,0:T(8,128)(2,1)S(1)} %copy-done.3, f32[768,64]{0,1:T(8,128)S(1)} %fusion.11), kind=kOutput, calls=%fused_computation.16 | convolution fusion | flops 402948096 | bytes 7110656 | tf_op jit(solution)/shard_map/dot_general | solution.py:131
  106.9 0.1 broadcast_in_dim.2
  107.0 52.2 %all_to_all.30 = bf16[16,768,64]{1,2,0:T(8,128)(2,1)S(1)} all-to-all(bf16[16,768,64]{1,2,0:T(8,128)(2,1)S(1)} %broadcast_in_dim.2), channel_id=1, replica_groups=mesh['ep'=32,'tp'=16] {'tp'}, dimensions={0} | all-to-all | bytes 3145728 | tf_op jit(solution)/shard_map/all_to_all | solution.py:19
  159.3 1.4 convolution_convert_fusion.2
  160.6 9.9 %all-to-all-start.2 = ((bf16[32,24,256]{2,1,0:T(8,128)(2,1)}), bf16[32,24,256]{2,1,0:T(8,128)(2,1)S(1)}, u32[]{:S(2)}, u32[]{:S(2)}) async-start(bf16[32,24,256]{2,1,0:T(8,128)(2,1)} %bitcast.17), calls=%async_computation.3 | async-start | bytes 786432 | tf_op jit(solution)/shard_map/all_to_all | solution.py:136
  170.6 11.8 %reduce-scatter.2.cloned.1.call-done = bf16[384,256]{1,0:T(8,128)(2,1)} async-done(((bf16[384,4096]{1,0:T(8,128)(2,1)}), bf16[384,256]{1,0:T(8,128)(2,1)}) %reduce-scatter.2.cloned.1.call-update) | async-done | bytes 196624 | tf_op jit(solution)/shard_map/reduce_scatter | solution.py:35
  182.4 1.6 slice.152
  183.9 1.3 all-to-all-done.2
  185.2 0.8 gather_fusion
  186.1 0.8 gather_fusion.1
  186.9 0.8 gather_fusion.2
  187.8 0.8 gather_fusion.3
  188.6 1.6 add_convert_fusion.2
  (46 shorter events, 0.6 us)
Async XLA Ops:
  7.2 41.8 %copy-start = (bf16[128,4096]{1,0:T(8,128)(2,1)S(1)}, bf16[128,4096]{1,0:T(8,128)(2,1)}, u32[]{:S(2)}) copy-start(bf16[128,4096]{1,0:T(8,128)(2,1)} %param.17) | copy-start | bytes 3145732
  7.2 5.1 %copy-start.2 = (bf16[128,4096]{1,0:T(8,128)(2,1)S(1)}, bf16[128,4096]{1,0:T(8,128)(2,1)}, u32[]{:S(2)}) copy-start(bf16[128,4096]{1,0:T(8,128)(2,1)} %param.18) | copy-start | bytes 3145732
  7.2 5.6 %copy-start.7 = (f32[4096]{0:T(1024)S(1)}, f32[4096]{0:T(1024)}, u32[]{:S(2)}) copy-start(f32[4096]{0:T(1024)} %param.19) | copy-start | bytes 49156
  7.2 92.6 %all-gather.2.cloned.1.call-start = ((), (), s32[]{:S(2)}) async-start(), calls=%async_computation.5 | async-start | bytes 6684672 | tf_op jit(solution)/shard_map/all_gather | solution.py:129
  12.8 29.6 %copy-start.6 = (bf16[256,128]{1,0:T(8,128)(2,1)S(1)}, bf16[256,128]{1,0:T(8,128)(2,1)}, u32[]{:S(2)}) copy-start(bf16[256,128]{1,0:T(8,128)(2,1)} %param.14) | copy-start | bytes 196612
  12.8 32.4 %copy-start.10 = (bf16[4096,32]{0,1:T(8,128)(2,1)S(1)}, bf16[4096,32]{0,1:T(8,128)(2,1)}, u32[]{:S(2)}) copy-start(bf16[4096,32]{0,1:T(8,128)(2,1)} %param.25) | copy-start | bytes 786436
  14.7 31.0 %copy-start.5 = (bf16[32,4096]{1,0:T(8,128)(2,1)S(1)}, bf16[32,4096]{1,0:T(8,128)(2,1)}, u32[]{:S(2)}) copy-start(bf16[32,4096]{1,0:T(8,128)(2,1)} %param.27) | copy-start | bytes 786436
  42.3 140.1 %reduce-scatter.2.cloned.1.call-start = ((), (), s32[]{:S(2)}) async-start(), calls=%async_computation.4 | async-start | bytes 3342336 | tf_op jit(solution)/shard_map/reduce_scatter | solution.py:35
  42.3 6.6 %collective-permute-start = (bf16[15,128]{1,0:T(8,128)(2,1)S(1)}, bf16[15,128]{1,0:T(8,128)(2,1)S(1)}, u32[]{:S(2)}, u32[]{:S(2)}) collective-permute-start(bf16[15,128]{1,0:T(8,128)(2,1)S(1)} %slice.88), channel_id=1, source_target_pairs={{0,16},{16,32},{32,48},{48,64},{64,80},{80,96},{96,112},{112,128},... | collective-permute-start | bytes 11528 | tf_op jit(solution)/shard_map/ppermute | solution.py:14
  55.8 44.0 %copy-start.4 = (bf16[1,4096,64]{1,2,0:T(8,128)(2,1)S(1)}, bf16[1,4096,64]{1,2,0:T(8,128)(2,1)}, u32[]{:S(2)}) copy-start(bf16[1,4096,64]{1,2,0:T(8,128)(2,1)} %param.22) | copy-start | bytes 1572868
  55.8 48.9 %copy-start.3 = (bf16[1,4096,64]{1,2,0:T(8,128)(2,1)S(1)}, bf16[1,4096,64]{1,2,0:T(8,128)(2,1)}, u32[]{:S(2)}) copy-start(bf16[1,4096,64]{1,2,0:T(8,128)(2,1)} %param.23) | copy-start | bytes 1572868
  99.8 5.0 %copy-start.1 = (bf16[768,4096]{1,0:T(8,128)(2,1)S(1)}, bf16[768,4096]{1,0:T(8,128)(2,1)}, u32[]{:S(2)}) copy-start(bf16[768,4096]{1,0:T(8,128)(2,1)} %all-gather.2.cloned.1.call-done) | copy-start | bytes 18874372
  106.9 52.4 %copy-start.9 = (bf16[1,1024,256]{2,1,0:T(8,128)(2,1)S(1)}, bf16[1,1024,256]{2,1,0:T(8,128)(2,1)}, u32[]{:S(2)}) copy-start(bf16[1,1024,256]{2,1,0:T(8,128)(2,1)} %param.24) | copy-start | bytes 1572868
  159.3 11.3 %copy-start.8 = (f32[128,4]{0,1:T(4,128)S(1)}, f32[128,4]{0,1:T(4,128)}, u32[]{:S(2)}) copy-start(f32[128,4]{0,1:T(4,128)} %param.21) | copy-start | bytes 6148
  160.6 24.6 %all-to-all-start.2 = ((bf16[32,24,256]{2,1,0:T(8,128)(2,1)}), bf16[32,24,256]{2,1,0:T(8,128)(2,1)S(1)}, u32[]{:S(2)}, u32[]{:S(2)}) async-start(bf16[32,24,256]{2,1,0:T(8,128)(2,1)} %bitcast.17), calls=%async_computation.3 | async-start | bytes 786432 | tf_op jit(solution)/shard_map/all_to_all | solution.py:136
Sparse Core Ops, SparseCore 0:
  42.4 57.3 all-gather.1
  102.7 79.6 reduce-scatter.1
where the time goes:
time: 198 us; the launch traced here: 197 us
  blocking collectives  79.7 us (40%)
  waiting for transfers between devices  57.1 us (29%)
  matrix products  16.5 us (8%)
  between operations  14.3 us (7%)
  starting transfers between devices  12.3 us (6%)
  other arithmetic  9.7 us (5%)
  local copies, waits for them, and re-layouts  7.53 us (4%)
    all_to_all x1, blocking collectives, sent_to_all(): lax.all_to_all(jnp.broadcast_to(x[None], (devices, *x.shape)), axis, 0, 0...  52.2 us
    all_gather x1, waiting for transfers between devices, per_device(): shard_cols = lax.all_gather(arrived, 'tp', axis=1, tiled=True)  44 us
    all_to_all x1, blocking collectives, per_device(): lax.all_to_all(my_slice, 'ep', split_axis=0, concat_axis=0, tiled=True)  27.4 us
    reduce_scatter x1, waiting for transfers between devices, in_one_piece(): lax.psum_scatter(both, axis, scatter_dimension=dim, tiled=True)  11.8 us
    all_to_all x1, starting transfers between devices, per_device(): lax.all_to_all(expert_result, 'ep', split_axis=0, concat_axis=0, tiled=True)  9.89 us
    dot_general x1, matrix products, per_device(): jnp.dot(shard_cols, gate_weight, preferred_element_type=jnp.float32)  4.96 us
  transfers between devices with their start and end apart: 4, of which 3 were waited for; matrix products, arithmetic and copies ran while one was open for 11% of the time, Pallas kernels for 0%

commit v1 on v0

--- a/solution.py
+++ b/solution.py
@@ -126,7 +126,8 @@
     slice_width = outgoing.shape[1] // lax.axis_size("tp")
     my_slice = lax.dynamic_slice_in_dim(outgoing, tp_rank * slice_width, slice_width, 1)
     arrived = lax.all_to_all(my_slice, "ep", split_axis=0, concat_axis=0, tiled=True)
-    shard_cols = lax.all_gather(arrived, "tp", axis=1, tiled=True)
+    stack = jnp.stack([arrived] * lax.axis_size("tp"))
+    shard_cols = jnp.concatenate(lax.all_to_all(stack, "tp", 0, 0), axis=1)
     gate_val = jnp.dot(shard_cols, gate_weight, preferred_element_type=jnp.float32)
     up_val = jnp.dot(shard_cols, up_weight, preferred_element_type=jnp.float32)
     hidden = (jax.nn.silu(gate_val) * up_val).astype(jnp.bfloat16)

time: 198 us -> 295 us (1.49)
  waiting for transfers between devices: 57.1 us -> 154 us
  blocking collectives: 79.7 us -> 72.7 us
  local copies, waits for them, and re-layouts: 7.53 us -> 11 us
  starting transfers between devices: 12.3 us -> 15.7 us
    all_to_all x0 -> x1, waiting for transfers between devices: none -> 140 us  [per_device(): shard_cols = jnp.concatenate(lax.all_to_all(stack, 'tp', 0, 0), axis=1)]
    all_gather x1 -> x0, waiting for transfers between devices: 44 us -> none  [per_device(): shard_cols = lax.all_gather(arrived, 'tp', axis=1, tiled=True)]
    all_to_all x1, waiting for transfers between devices: 1.29 us -> 13.2 us  [per_device(): lax.all_to_all(expert_result, 'ep', split_axis=0, concat_axis=0, tiled=True)]
    reduce_scatter x1, waiting for transfers between devices: 11.8 us -> 0.02 us  [in_one_piece(): lax.psum_scatter(both, axis, scatter_dimension=dim, tiled=True)]
    all_to_all x0 -> x1, starting transfers between devices: none -> 9.66 us  [per_device(): shard_cols = jnp.concatenate(lax.all_to_all(stack, 'tp', 0, 0), axis=1)]
    all_to_all x1, blocking collectives: 52.2 us -> 45.4 us  [sent_to_all(): lax.all_to_all(jnp.broadcast_to(x[None], (devices, *x.shape)), axis, 0, 0...]
    all_to_all x1, starting transfers between devices: 9.89 us -> 3.88 us  [per_device(): lax.all_to_all(expert_result, 'ep', split_axis=0, concat_axis=0, tiled=True)]
    another operation x1 -> x3, local copies, waits for them, and re-layouts: 0.01 us -> 3.43 us  [the longest x2 3.43 us: per_device(): stack = jnp.stack([arrived] * lax.axis_size('tp'))]
  transfers between devices with their start and end apart: 4 -> 4, of which waited for: 3 -> 2; matrix products, arithmetic and copies ran while one was open for 11% -> 8% of each run, Pallas kernels for 0% -> 0%
where the time goes in v1:
time: 295 us; the launch traced here: 294 us
  waiting for transfers between devices  154 us (52%)
  blocking collectives  72.7 us (25%)
  matrix products  17.5 us (6%)
  starting transfers between devices  15.7 us (5%)
  between operations  14.3 us (5%)
  local copies, waits for them, and re-layouts  11 us (4%)
  other arithmetic  9.63 us (3%)
    all_to_all x1, waiting for transfers between devices, per_device(): shard_cols = jnp.concatenate(lax.all_to_all(stack, 'tp', 0, 0), axis=1)  140 us
    all_to_all x1, blocking collectives, sent_to_all(): lax.all_to_all(jnp.broadcast_to(x[None], (devices, *x.shape)), axis, 0, 0...  45.4 us
    all_to_all x1, blocking collectives, per_device(): lax.all_to_all(my_slice, 'ep', split_axis=0, concat_axis=0, tiled=True)  27.3 us
    all_to_all x1, waiting for transfers between devices, per_device(): lax.all_to_all(expert_result, 'ep', split_axis=0, concat_axis=0, tiled=True)  13.2 us
    all_to_all x1, starting transfers between devices, per_device(): shard_cols = jnp.concatenate(lax.all_to_all(stack, 'tp', 0, 0), axis=1)  9.66 us
  transfers between devices with their start and end apart: 4, of which 2 were waited for; matrix products, arithmetic and copies ran while one was open for 8% of the time, Pallas kernels for 0%

profile of v1, /device:TPU:1, one launch (start us, length us, event | category | flops | bytes accessed | tf_op | source)
XLA Modules:
  0.0 294.4 jit_solution(17946289315237139592)
XLA Ops:
  7.2 0.9 copy.28
  8.4 1.2 reduce-window.6
  9.5 0.2 slice_reduce_fusion
  10.1 0.7 multiply_add_fusion
  10.8 1.5 convert_reduce_fusion
  12.3 0.4 fusion.2
  12.7 2.0 fusion.13
  14.8 27.3 %all_to_all.31 = bf16[32,24,256]{2,1,0:T(8,128)(2,1)S(1)} all-to-all(bf16[32,24,256]{2,1,0:T(8,128)(2,1)S(1)} %bitcast.91), channel_id=1, replica_groups=mesh['ep'=32,'tp'=16] {'ep'}, dimensions={0} | all-to-all | bytes 786432 | tf_op jit(solution)/shard_map/all_to_all | solution.py:128
  42.1 0.2 copy.32
  42.3 3.3 %stack.5 = bf16[16,768,256]{1,2,0:T(8,128)(2,1)} broadcast(bf16[768,256]{0,1:T(8,128)(2,1)S(1)} %copy.32), dimensions={1,2} | broadcast | bytes 6684672 | tf_op jit(solution)/shard_map/stack | solution.py:129
  45.5 9.7 %all-to-all-start.1 = ((bf16[16,768,256]{1,2,0:T(8,128)(2,1)}), bf16[16,768,256]{1,2,0:T(8,128)(2,1)}, u32[]{:S(2)}, u32[]{:S(2)}) async-start(bf16[16,768,256]{1,2,0:T(8,128)(2,1)} %stack.5), calls=%async_computation.2 | async-start | bytes 12582912 | tf_op jit(solution)/shard_map/all_to_all | solution.py:130
  55.3 2.1 collective-permute-start
  57.4 0.5 compare_convert_fusion
  58.0 0.5 fusion.102
  58.5 2.4 convolution_convert_fusion.1
  60.9 0.8 dynamic_slice.10
  61.7 3.2 %convolution_convert_fusion = bf16[256,4096]{1,0:T(8,128)(2,1)} fusion(bf16[128,4096]{1,0:T(8,128)(2,1)S(1)} %copy-done, f32[256,128]{1,0:T(8,128)S(1)} %convert_element_type.122, f32[15,128]{1,0:T(8,128)S(1)} %convert_element_type.124, f32[128]{0:T(128)S(1)} %dynamic_slice.10, f32[256]{0:T(256)S(1)} %get-tuple-element.18, f32[128]{0:T(128)} %get-tuple-element.14, ...), kind=kOutput, calls=%fused_computation.4 | convolution fusion | flops 279379968 | bytes 3323908 | tf_op jit(solution)/shard_map/dot_general | solution.py:74
  65.0 3.5 %pad_maximum_fusion = bf16[384,4096]{1,0:T(8,128)(2,1)} fusion(bf16[128,4096]{1,0:T(8,128)(2,1)S(1)} %convolution_convert_fusion.1, bf16[256,4096]{1,0:T(8,128)(2,1)} %convolution_convert_fusion), kind=kLoop, calls=%fused_computation.6 | loop fusion | flops 6291456 | bytes 6291456 | tf_op jit(solution)/shard_map/concatenate | solution.py:34
  68.5 140.3 %all-to-all-done.1 = bf16[16,768,256]{1,2,0:T(8,128)(2,1)} async-done(((bf16[16,768,256]{1,2,0:T(8,128)(2,1)}), bf16[16,768,256]{1,2,0:T(8,128)(2,1)}, u32[]{:S(2)}, u32[]{:S(2)}) %all-to-all-start.1) | async-done | bytes 6291488 | tf_op jit(solution)/shard_map/all_to_all | solution.py:130
  208.8 4.0 %fusion.11 = f32[768,64]{0,1:T(8,128)S(1)} fusion(bf16[768,4096]{0,1:T(8,128)(2,1)} %bitcast.13, bf16[1,4096,64]{1,2,0:T(8,128)(2,1)S(1)} %copy-done.3), kind=kOutput, calls=%fused_computation.39 | convolution fusion | flops 402653184 | bytes 7012352 | tf_op jit(solution)/shard_map/dot_general | solution.py:131
  212.8 4.0 %fusion.5 = bf16[768,64]{0,1:T(8,128)(2,1)S(1)} fusion(bf16[768,4096]{0,1:T(8,128)(2,1)} %bitcast.13, bf16[1,4096,64]{1,2,0:T(8,128)(2,1)S(1)} %copy-done.2, f32[768,64]{0,1:T(8,128)S(1)} %fusion.11), kind=kOutput, calls=%fused_computation.16 | convolution fusion | flops 402948096 | bytes 7110656 | tf_op jit(solution)/shard_map/dot_general | solution.py:132
  216.8 0.1 broadcast_in_dim.2
  217.0 45.4 %all_to_all.32 = bf16[16,768,64]{1,2,0:T(8,128)(2,1)S(1)} all-to-all(bf16[16,768,64]{1,2,0:T(8,128)(2,1)S(1)} %broadcast_in_dim.2), channel_id=1, replica_groups=mesh['ep'=32,'tp'=16] {'tp'}, dimensions={0} | all-to-all | bytes 3145728 | tf_op jit(solution)/shard_map/all_to_all | solution.py:19
  262.4 1.4 convolution_convert_fusion.2
  263.8 3.9 %all-to-all-start.3 = ((bf16[32,24,256]{2,1,0:T(8,128)(2,1)}), bf16[32,24,256]{2,1,0:T(8,128)(2,1)S(1)}, u32[]{:S(2)}, u32[]{:S(2)}) async-start(bf16[32,24,256]{2,1,0:T(8,128)(2,1)} %bitcast.20), calls=%async_computation.4 | async-start | bytes 786432 | tf_op jit(solution)/shard_map/all_to_all | solution.py:137
  267.8 1.6 slice.152
  269.3 13.2 %all-to-all-done.3 = bf16[32,24,256]{2,1,0:T(8,128)(2,1)S(1)} async-done(((bf16[32,24,256]{2,1,0:T(8,128)(2,1)}), bf16[32,24,256]{2,1,0:T(8,128)(2,1)S(1)}, u32[]{:S(2)}, u32[]{:S(2)}) %all-to-all-start.3) | async-done | bytes 393248 | tf_op jit(solution)/shard_map/all_to_all | solution.py:137
  282.6 0.8 gather_fusion
  283.4 0.8 gather_fusion.1
  284.3 0.8 gather_fusion.2
  285.1 0.8 gather_fusion.3
  286.0 1.6 add_convert_fusion.2
  (45 shorter events, 0.8 us)
Async XLA Ops:
  7.2 54.6 %copy-start = (bf16[128,4096]{1,0:T(8,128)(2,1)S(1)}, bf16[128,4096]{1,0:T(8,128)(2,1)}, u32[]{:S(2)}) copy-start(bf16[128,4096]{1,0:T(8,128)(2,1)} %param.17) | copy-start | bytes 3145732
  7.2 5.1 %copy-start.1 = (bf16[128,4096]{1,0:T(8,128)(2,1)S(1)}, bf16[128,4096]{1,0:T(8,128)(2,1)}, u32[]{:S(2)}) copy-start(bf16[128,4096]{1,0:T(8,128)(2,1)} %param.18) | copy-start | bytes 3145732
  7.2 5.5 %copy-start.6 = (f32[4096]{0:T(1024)S(1)}, f32[4096]{0:T(1024)}, u32[]{:S(2)}) copy-start(f32[4096]{0:T(1024)} %param.19) | copy-start | bytes 49156
  45.5 9.7 %copy-start.5 = (bf16[256,128]{1,0:T(8,128)(2,1)S(1)}, bf16[256,128]{1,0:T(8,128)(2,1)}, u32[]{:S(2)}) copy-start(bf16[256,128]{1,0:T(8,128)(2,1)} %param.14) | copy-start | bytes 196612
  45.5 12.4 %copy-start.9 = (bf16[4096,32]{0,1:T(8,128)(2,1)S(1)}, bf16[4096,32]{0,1:T(8,128)(2,1)}, u32[]{:S(2)}) copy-start(bf16[4096,32]{0,1:T(8,128)(2,1)} %param.25) | copy-start | bytes 786436
  45.5 163.3 %all-to-all-start.1 = ((bf16[16,768,256]{1,2,0:T(8,128)(2,1)}), bf16[16,768,256]{1,2,0:T(8,128)(2,1)}, u32[]{:S(2)}, u32[]{:S(2)}) async-start(bf16[16,768,256]{1,2,0:T(8,128)(2,1)} %stack.5), calls=%async_computation.2 | async-start | bytes 12582912 | tf_op jit(solution)/shard_map/all_to_all | solution.py:130
  55.2 3.3 %copy-start.4 = (bf16[32,4096]{1,0:T(8,128)(2,1)S(1)}, bf16[32,4096]{1,0:T(8,128)(2,1)}, u32[]{:S(2)}) copy-start(bf16[32,4096]{1,0:T(8,128)(2,1)} %param.27) | copy-start | bytes 786436
  55.2 212.6 %reduce-scatter.2.cloned.1.call-start = ((), (), s32[]{:S(2)}) async-start(), calls=%async_computation.5 | async-start | bytes 3342336 | tf_op jit(solution)/shard_map/reduce_scatter | solution.py:35
  55.3 6.5 %collective-permute-start = (bf16[15,128]{1,0:T(8,128)(2,1)S(1)}, bf16[15,128]{1,0:T(8,128)(2,1)S(1)}, u32[]{:S(2)}, u32[]{:S(2)}) collective-permute-start(bf16[15,128]{1,0:T(8,128)(2,1)S(1)} %slice.88), channel_id=1, source_target_pairs={{0,16},{16,32},{32,48},{48,64},{64,80},{80,96},{96,112},{112,128},... | collective-permute-start | bytes 11528 | tf_op jit(solution)/shard_map/ppermute | solution.py:14
  68.5 140.3 %copy-start.3 = (bf16[1,4096,64]{1,2,0:T(8,128)(2,1)S(1)}, bf16[1,4096,64]{1,2,0:T(8,128)(2,1)}, u32[]{:S(2)}) copy-start(bf16[1,4096,64]{1,2,0:T(8,128)(2,1)} %param.22) | copy-start | bytes 1572868
  208.8 4.0 %copy-start.2 = (bf16[1,4096,64]{1,2,0:T(8,128)(2,1)S(1)}, bf16[1,4096,64]{1,2,0:T(8,128)(2,1)}, u32[]{:S(2)}) copy-start(bf16[1,4096,64]{1,2,0:T(8,128)(2,1)} %param.23) | copy-start | bytes 1572868
  216.8 45.6 %copy-start.8 = (bf16[1,1024,256]{2,1,0:T(8,128)(2,1)S(1)}, bf16[1,1024,256]{2,1,0:T(8,128)(2,1)}, u32[]{:S(2)}) copy-start(bf16[1,1024,256]{2,1,0:T(8,128)(2,1)} %param.24) | copy-start | bytes 1572868
  262.4 5.3 %copy-start.7 = (f32[128,4]{0,1:T(4,128)S(1)}, f32[128,4]{0,1:T(4,128)}, u32[]{:S(2)}) copy-start(f32[128,4]{0,1:T(4,128)} %param.21) | copy-start | bytes 6148
  263.8 18.8 %all-to-all-start.3 = ((bf16[32,24,256]{2,1,0:T(8,128)(2,1)}), bf16[32,24,256]{2,1,0:T(8,128)(2,1)S(1)}, u32[]{:S(2)}, u32[]{:S(2)}) async-start(bf16[32,24,256]{2,1,0:T(8,128)(2,1)} %bitcast.20), calls=%async_computation.4 | async-start | bytes 786432 | tf_op jit(solution)/shard_map/all_to_all | solution.py:137
Sparse Core Ops, SparseCore 0:
  68.6 139.9 reduce-scatter.1
